TPU v7x, 256 devices: a 4x2x16 block of a 4x16x16 slice. The times are simulated.
256 devices in a mesh: grp: 2 (over y), sp: 32 (over z, core), tp: 4 (over x).
Axes of the slice: x: 4, y: 2, z: 16, core: 2. Of those that a mesh axis runs over, the one named last changes fastest.
The devices are a block of a 4x16x16 slice.
Arguments:
- mix_in: bfloat16 [16384, 1536], P(('grp', 'sp'), 'tp'), parts along dimension 0, may hold values from -6 to 6
- resid_in: bfloat16 [16384, 2048], P(('grp', 'sp', 'tp')), parts along dimension 0, may hold values from -6 to 6
- doc_ids: int32 [16384], P(('grp', 'sp')), parts along dimension 0, may hold values from 0 to 15, never falling along the last dimension, each value on 1 to 768 neighbouring positions
- group_weight: bfloat16 [4, 384, 384], P('tp'), may hold values from -0.3125 to 0.3125
- pool_scale: float32 [1536], P('tp'), may hold values from 0.1 to 1.9
- out_weight: bfloat16 [1536, 2048], P('tp'), may hold values from -0.15625 to 0.15625
- norm_gain: float32 [2048], replicated, may hold values from 0.1 to 1.9
- expert_ids: int32 [16384, 2], P(('grp', 'sp', 'tp')), parts along dimension 0, may hold values from 0 to 127, as said below
- route_weights: float32 [16384, 2], P(('grp', 'sp', 'tp')), parts along dimension 0, may hold values from 0.1 to 1
- w_gate: bfloat16 [128, 2048, 512], P(('sp', 'tp')), may hold values from -0.125 to 0.125
- w_up: bfloat16 [128, 2048, 512], P(('sp', 'tp')), may hold values from -0.125 to 0.125
- w_down: bfloat16 [128, 512, 2048], P(('sp', 'tp')), may hold values from -0.25 to 0.25
Outputs:
- layer_out: bfloat16 [16384, 2048], P(('grp', 'sp', 'tp')), parts along dimension 0
There are 2 independent parts, one for each index of `grp`. A program takes and returns all parts, laid end to end along the dimension named above; an argument that names none is the same for every part. Nothing has to cross between parts.
Inputs may be any that keep to these rules, and one draw needn't show every extreme that they name: `doc_ids`: document numbers never fall along the positions. `expert_ids`: each row names two different experts of one group of 32 consecutive experts. Among the rows of one device (aligned blocks of 64 rows) no expert is named more than 2 times; in every draw the experts of some group are each named exactly 2 times in every block.
All inputs are finite; a program needn't handle non-finite values.
Results may differ from a plain program's by a relative error of at most 0.012.
Values may be sent and summed in bfloat16 or wider, within the bound.
A program may use at most 64 MiB of HBM per device.

v0:
```python
import jax
import jax.numpy as jnp
from jax import lax
from jax.sharding import PartitionSpec as P

HALO = 16
TOP_K = 2


def from_behind(value, axis, steps):
    count = lax.axis_size(axis)
    leading, last = (max(0, -steps), min(count, count - steps))
    return lax.ppermute(value, axis, [(source, source + steps) for source in range(leading, last)])


def cut_along(shard, dim, peers):
    before, after = (shard.shape[:dim], shard.shape[dim + 1 :])
    return jnp.moveaxis(shard.reshape(*before, peers, -1, *after), dim, 0)


def sum_at_owner(shard, axis, dim):
    peers = lax.axis_size(axis)
    pieces = lax.all_to_all(cut_along(shard, dim, peers), axis, 0, 0, tiled=True)
    return jnp.sum(pieces, axis=0)


def expert_rows(flat_rows, w_gate, w_up, w_down):
    gate_part = jnp.dot(flat_rows, w_gate[0], preferred_element_type=jnp.float32)
    up_part = jnp.dot(flat_rows, w_up[0], preferred_element_type=jnp.float32)
    hidden = (jax.nn.silu(gate_part) * up_part).astype(jnp.bfloat16)
    return jnp.dot(hidden, w_down[0], preferred_element_type=jnp.float32).astype(jnp.bfloat16)


def shards(
    mix_in,
    resid_in,
    doc_ids,
    group_weight,
    pool_scale,
    out_weight,
    norm_gain,
    expert_ids,
    route_weights,
    w_gate,
    w_up,
    w_down,
):
    local_rows, group_width = mix_in.shape
    reach = jnp.left_shift(jnp.int32(2), lax.axis_index("tp"))
    marked = doc_ids + 1
    prior_rows, prior_marks = from_behind(
        (mix_in[local_rows - HALO :], marked[local_rows - HALO :]), "sp", 1
    )
    extended = jnp.concatenate([prior_rows, mix_in], axis=0).astype(jnp.float32)
    ext_marks = jnp.concatenate([prior_marks, marked], axis=0)
    running = jnp.zeros((local_rows, group_width), jnp.float32)
    members = jnp.zeros((local_rows,), jnp.float32)
    for offset in range(HALO):
        rows_back = extended[HALO - offset : HALO - offset + local_rows]
        keep = (ext_marks[HALO - offset : HALO - offset + local_rows] == marked) & (offset < reach)
        running = running + jnp.where(keep[:, None], rows_back, 0.0)
        members = members + keep.astype(jnp.float32)
    mixed = (running / members[:, None] - mix_in.astype(jnp.float32)).astype(jnp.bfloat16)
    grouped = (
        jnp.dot(mixed, group_weight[0], preferred_element_type=jnp.float32) * pool_scale
    ).astype(jnp.bfloat16)
    tp_size = lax.axis_size("tp")
    token_rows = local_rows // tp_size
    projected = sum_at_owner(
        jnp.dot(grouped, out_weight, preferred_element_type=jnp.float32), "tp", 0
    )
    stream_f = (resid_in.astype(jnp.float32) + projected).astype(jnp.bfloat16).astype(jnp.float32)
    level = jnp.mean(stream_f * stream_f, axis=1, keepdims=True)
    normed = (stream_f * lax.rsqrt(level + 1e-06) * norm_gain).astype(jnp.bfloat16)
    sp_size = lax.axis_size("sp")
    expert_count = sp_size * tp_size
    capacity = max(2, 4 * token_rows // expert_count)
    width = normed.shape[1]
    route_expert = expert_ids.reshape(-1)
    onehot = (route_expert[:, None] == jnp.arange(expert_count, dtype=jnp.int32)[None, :]).astype(
        jnp.int32
    )
    slot_index = jnp.sum(onehot * (jnp.cumsum(onehot, axis=0) - 1), axis=1)
    target = route_expert * capacity + slot_index
    source_rows = jnp.repeat(normed, TOP_K, axis=0)
    outbox = jnp.zeros((expert_count * capacity, width), jnp.bfloat16).at[target].set(source_rows)
    arrived = lax.all_to_all(
        outbox.reshape(expert_count, capacity, width),
        ("sp", "tp"),
        split_axis=0,
        concat_axis=0,
        tiled=True,
    )
    served = expert_rows(arrived.reshape(-1, width), w_gate, w_up, w_down).reshape(arrived.shape)
    returned = lax.all_to_all(served, ("sp", "tp"), split_axis=0, concat_axis=0, tiled=True)
    answers = returned.reshape(expert_count * capacity, width)[target].astype(jnp.float32)
    weighted = answers * route_weights.reshape(-1)[:, None]
    paired = weighted.reshape(token_rows, TOP_K, width)
    return (stream_f + paired[:, 0] + paired[:, 1]).astype(jnp.bfloat16)


def solution(mesh):
    return jax.shard_map(
        shards,
        mesh=mesh,
        in_specs=(
            P(("grp", "sp"), "tp"),
            P(("grp", "sp", "tp"), None),
            P(("grp", "sp")),
            P("tp", None, None),
            P("tp"),
            P("tp", None),
            P(),
            P(("grp", "sp", "tp"), None),
            P(("grp", "sp", "tp"), None),
            P(("sp", "tp"), None, None),
            P(("sp", "tp"), None, None),
            P(("sp", "tp"), None, None),
        ),
        out_specs=P(("grp", "sp", "tp"), None),
        check_vma=False,
    )
```

profile of v0, /device:TPU:40, one launch (start us, length us, event | category | flops | bytes accessed | tf_op | source)
XLA Modules:
  0.0 215.0 jit_solution(5375581872212817277)
XLA Ops:
  0.0 0.0 copy-start
  0.0 0.8 broadcast_add_fusion
  0.8 0.1 slice.107
  0.9 1.8 collective-permute-start.1
  2.7 0.7 slice.105
  3.5 4.9 %collective-permute-start = (bf16[16,384]{1,0:T(8,128)(2,1)S(1)}, bf16[16,384]{1,0:T(8,128)(2,1)S(1)}, u32[]{:S(2)}, u32[]{:S(2)}) collective-permute-start(bf16[16,384]{1,0:T(8,128)(2,1)S(1)} %slice.105), channel_id=1, source_target_pairs={{0,4},{4,8},{8,12},{12,16},{16,20},{20,24},{24,28},{28,32},{32,36}... | collective-permute-start | bytes 36872 | tf_op jit(solution)/shard_map/ppermute | solution.py:13
  8.4 0.0 collective-permute-done.1
  8.4 0.1 pad_add_fusion
  8.5 0.8 convert_add_fusion.1
  9.3 0.0 collective-permute-done
  9.3 1.0 maximum_convert_fusion
  10.3 4.7 %fusion.12 = f32[256,2048]{1,0:T(8,128)} fusion(bf16[384,2048]{1,0:T(8,128)(2,1)} %param.17, bf16[1,384,384]{2,1,0:T(8,128)(2,1)} %param.15, bf16[256,384]{1,0:T(8,128)(2,1)} %param.12, f32[272,384]{1,0:T(8,128)S(1)} %maximum_convert_fusion, f32[384]{0:T(512)} %param.16, f32[256]{0:T(256)S(1)} %get-tuple-element.7, ...), kind=kOutput, calls=%fused_computation.12 | convolution fusion | flops 481787904 | bytes 10463233 | tf_op jit(solution)/shard_map/dot_general | solution.py:70
  15.0 0.0 copy-start.4
  15.0 4.7 %all-to-all-start = ((f32[4,64,2048]{2,1,0:T(8,128)}), f32[4,64,2048]{2,1,0:T(8,128)}, u32[]{:S(2)}, u32[]{:S(2)}) async-start(f32[4,64,2048]{2,1,0:T(8,128)} %bitcast.37), calls=%async_computation | async-start | bytes 4194304 | tf_op jit(solution)/shard_map/all_to_all | solution.py:23
  19.7 0.0 copy-done.4
  19.7 0.1 copy.17
  19.8 0.1 eq.75
  19.9 0.1 fusion.87
  20.0 0.2 reduce_window_sum.11
  20.2 0.1 copy.16
  20.3 0.1 mul.66
  20.4 0.2 select_reduce_fusion
  20.6 26.1 %all-to-all-done = f32[4,64,2048]{2,1,0:T(8,128)} async-done(((f32[4,64,2048]{2,1,0:T(8,128)}), f32[4,64,2048]{2,1,0:T(8,128)}, u32[]{:S(2)}, u32[]{:S(2)}) %all-to-all-start) | async-done | bytes 2097184 | tf_op jit(solution)/shard_map/all_to_all | solution.py:23
  46.7 1.8 reduce_sum.29
  48.5 0.0 copy-done.2
  48.5 0.2 fusion.15
  48.7 0.0 copy-done.3
  48.7 0.1 fusion.17
  48.8 0.3 broadcast_in_dim.149
  49.2 1.0 reshape.103
  50.1 2.2 %scatter_custom_fusion = bf16[256,2048]{1,0:T(8,128)(2,1)S(1)} fusion(s32[128]{0:T(128)S(1)} %fusion.88, bf16[128,2048]{1,0:T(8,128)(2,1)} %reshape.103, bf16[]{:T(256)} %constant.20.clone.1), kind=kCustom, calls=%fused_computation.29 | custom fusion | bytes 1049088 | tf_op jit(solution)/shard_map/scatter | solution.py:86
  52.4 1.5 reshape.86
  53.9 80.8 %all_to_all.15 = bf16[128,2,2048]{2,1,0:T(2,128)(2,1)S(1)} all-to-all(bf16[128,2,2048]{2,1,0:T(2,128)(2,1)} %reshape.86), channel_id=1, replica_groups=mesh['grp'=2,'sp'=32,'tp'=4] {'sp','tp'}, dimensions={0} | all-to-all | bytes 2097152 | tf_op jit(solution)/shard_map/all_to_all | solution.py:87
  134.6 1.2 reshape.87
  135.8 3.5 %fusion.3 = f32[256,512]{1,0:T(8,128)} fusion(bf16[256,2048]{1,0:T(8,128)(2,1)} %reshape.87, bf16[1,2048,512]{2,1,0:T(8,128)(2,1)} %param.21), kind=kOutput, calls=%fused_computation.6 | convolution fusion | flops 536870912 | bytes 3670016 | tf_op jit(solution)/shard_map/dot_general | solution.py:28
  139.4 0.0 copy-done
  139.4 0.0 copy-done.1
  139.4 4.0 %convolution_convert_fusion = bf16[256,2048]{1,0:T(8,128)(2,1)} fusion(bf16[1,512,2048]{2,1,0:T(8,128)(2,1)S(1)} %copy-done, bf16[256,2048]{1,0:T(8,128)(2,1)S(1)} %copy-done.1, bf16[1,2048,512]{2,1,0:T(8,128)(2,1)} %param.22, f32[256,512]{1,0:T(8,128)} %fusion.3), kind=kOutput, calls=%fused_computation.2 | convolution fusion | flops 1075052544 | bytes 6815744 | tf_op jit(solution)/shard_map/dot_general | solution.py:31
  143.4 2.5 %reshape.88 = bf16[128,2,2048]{2,1,0:T(2,128)(2,1)} reshape(bf16[256,2048]{1,0:T(8,128)(2,1)} %convolution_convert_fusion) | data formatting | bytes 2097152 | tf_op jit(solution)/shard_map/reshape | solution.py:94
  145.9 10.8 %all-to-all-start.2 = ((bf16[128,2,2048]{2,1,0:T(2,128)(2,1)}), bf16[128,2,2048]{2,1,0:T(2,128)(2,1)}, u32[]{:S(2)}, u32[]{:S(2)}) async-start(bf16[128,2,2048]{2,1,0:T(2,128)(2,1)} %reshape.88), calls=%async_computation.2 | async-start | bytes 2097152 | tf_op jit(solution)/shard_map/all_to_all | solution.py:95
  156.7 52.0 %all-to-all-done.2 = bf16[128,2,2048]{2,1,0:T(2,128)(2,1)} async-done(((bf16[128,2,2048]{2,1,0:T(2,128)(2,1)}), bf16[128,2,2048]{2,1,0:T(2,128)(2,1)}, u32[]{:S(2)}, u32[]{:S(2)}) %all-to-all-start.2) | async-done | bytes 1048608 | tf_op jit(solution)/shard_map/all_to_all | solution.py:95
  208.7 1.5 reshape.89
  210.1 0.0 copy-start.5
  210.2 1.7 gather_fusion
  211.9 1.7 reshape.90
  213.6 0.0 copy-done.5
  213.6 0.6 copy_multiply_fusion
  214.2 0.8 fusion.19
  (7 shorter events, 0.0 us)
Async XLA Ops:
  0.0 139.4 %copy-start = (bf16[1,512,2048]{2,1,0:T(8,128)(2,1)S(1)}, bf16[1,512,2048]{2,1,0:T(8,128)(2,1)}, u32[]{:S(2)}) copy-start(bf16[1,512,2048]{2,1,0:T(8,128)(2,1)} %param.23) | copy-start | bytes 6291460
  0.9 7.5 %collective-permute-start.1 = (s32[16]{0:T(128)S(1)}, s32[16]{0:T(128)S(1)}, u32[]{:S(2)}, u32[]{:S(2)}) collective-permute-start(s32[16]{0:T(128)S(1)} %slice.107), channel_id=1, source_target_pairs={{0,4},{4,8},{8,12},{12,16},{16,20},{20,24},{24,28},{28,32},{32,36}... | collective-permute-start | bytes 200 | tf_op jit(solution)/shard_map/ppermute | solution.py:13
  3.5 5.8 %collective-permute-start = (bf16[16,384]{1,0:T(8,128)(2,1)S(1)}, bf16[16,384]{1,0:T(8,128)(2,1)S(1)}, u32[]{:S(2)}, u32[]{:S(2)}) collective-permute-start(bf16[16,384]{1,0:T(8,128)(2,1)S(1)} %slice.105), channel_id=1, source_target_pairs={{0,4},{4,8},{8,12},{12,16},{16,20},{20,24},{24,28},{28,32},{32,36}... | collective-permute-start | bytes 36872 | tf_op jit(solution)/shard_map/ppermute | solution.py:13
  15.0 4.7 %copy-start.4 = (s32[64,2]{0,1:T(2,128)S(1)}, s32[64,2]{0,1:T(2,128)}, u32[]{:S(2)}) copy-start(s32[64,2]{0,1:T(2,128)} %param.19) | copy-start | bytes 1540
  15.0 31.8 %all-to-all-start = ((f32[4,64,2048]{2,1,0:T(8,128)}), f32[4,64,2048]{2,1,0:T(8,128)}, u32[]{:S(2)}, u32[]{:S(2)}) async-start(f32[4,64,2048]{2,1,0:T(8,128)} %bitcast.37), calls=%async_computation | async-start | bytes 4194304 | tf_op jit(solution)/shard_map/all_to_all | solution.py:23
  19.7 28.8 %copy-start.2 = (bf16[64,2048]{1,0:T(8,128)(2,1)S(1)}, bf16[64,2048]{1,0:T(8,128)(2,1)}, u32[]{:S(2)}) copy-start(bf16[64,2048]{1,0:T(8,128)(2,1)} %param.13) | copy-start | bytes 786436
  19.7 29.0 %copy-start.3 = (f32[2048]{0:T(1024)S(1)}, f32[2048]{0:T(1024)}, u32[]{:S(2)}) copy-start(f32[2048]{0:T(1024)} %param.18) | copy-start | bytes 24580
  135.8 3.5 %copy-start.1 = (bf16[256,2048]{1,0:T(8,128)(2,1)S(1)}, bf16[256,2048]{1,0:T(8,128)(2,1)}, u32[]{:S(2)}) copy-start(bf16[256,2048]{1,0:T(8,128)(2,1)} %reshape.87) | copy-start | bytes 3145732
  145.9 62.8 %all-to-all-start.2 = ((bf16[128,2,2048]{2,1,0:T(2,128)(2,1)}), bf16[128,2,2048]{2,1,0:T(2,128)(2,1)}, u32[]{:S(2)}, u32[]{:S(2)}) async-start(bf16[128,2,2048]{2,1,0:T(2,128)(2,1)} %reshape.88), calls=%async_computation.2 | async-start | bytes 2097152 | tf_op jit(solution)/shard_map/all_to_all | solution.py:95
  210.1 3.4 %copy-start.5 = (f32[64,2]{0,1:T(2,128)S(1)}, f32[64,2]{0,1:T(2,128)}, u32[]{:S(2)}) copy-start(f32[64,2]{0,1:T(2,128)} %param.20) | copy-start | bytes 1540
where the time goes:
time: 217 us; the launch traced here: 215 us
  blocking collectives  80.8 us (37%)
  waiting for transfers between devices  78.1 us (36%)
  starting transfers between devices  22.2 us (10%)
  local copies, waits for them, and re-layouts  14.9 us (7%)
  matrix products  12.2 us (6%)
  other arithmetic  6.56 us (3%)
    all_to_all x1, blocking collectives, shards(): lax.all_to_all(outbox.reshape(expert_count, capacity, width), ('sp', 'tp'...  80.8 us
    all_to_all x1, waiting for transfers between devices, shards(): lax.all_to_all(served, ('sp', 'tp'), split_axis=0, concat_axis=0, tiled=T...  52 us
    all_to_all x1, waiting for transfers between devices, sum_at_owner(): lax.all_to_all(cut_along(shard, dim, peers), axis, 0, 0, tiled=True)  26.1 us
    all_to_all x1, starting transfers between devices, shards(): lax.all_to_all(served, ('sp', 'tp'), split_axis=0, concat_axis=0, tiled=T...  10.8 us
    ppermute x2, starting transfers between devices, from_behind(): lax.ppermute(value, axis, [(source, source + steps) for source in range(l...  6.74 us
    dot_general x1, matrix products, shards(): jnp.dot(grouped, out_weight, preferred_element_type=jnp.float32)  4.71 us
    all_to_all x1, starting transfers between devices, sum_at_owner(): lax.all_to_all(cut_along(shard, dim, peers), axis, 0, 0, tiled=True)  4.71 us
  transfers between devices with their start and end apart: 4, of which 2 were waited for; matrix products, arithmetic and copies ran while one was open for 1% of the time, Pallas kernels for 0%

commit v1 on v0

v1 whole, which is shorter than its diff:
```python
import jax
import jax.numpy as jnp
from jax import lax
from jax.experimental import pallas as pl
from jax.experimental.pallas import tpu as pltpu
from jax.sharding import PartitionSpec as P

MESH = pl.DeviceIdType.MESH
BF = jnp.bfloat16
F32 = jnp.float32
HALO = 16
EPG = 32
CAP = 2
NB = 4


def dot(a, b):
    return lax.dot_general(a, b, (((1,), (0,)), ((), ())), preferred_element_type=F32)


def dot_t(a, b):
    return lax.dot_general(a, b, (((0,), (0,)), ((), ())), preferred_element_type=F32)


def iota(shape, dim):
    return lax.broadcasted_iota(jnp.int32, shape, dim)


def drain(ref, sem):
    pltpu.make_async_copy(ref, ref, sem).wait()


def kernel(
    sp_size,
    tp_size,
    mix_hbm,
    resid_hbm,
    doc_ref,
    gw_hbm,
    scale_ref,
    ow_hbm,
    gain_ref,
    ids_ref,
    rw_ref,
    wg_hbm,
    wu_hbm,
    wd_hbm,
    out_ref,
    mix_v,
    halo_v,
    hdoc_v,
    resid_v,
    gw_v,
    ow_v,
    wg_v,
    wu_v,
    wd_v,
    mixed_v,
    grouped_v,
    s1_out,
    s1_in,
    s2_out,
    s2_in,
    stream_v,
    a_out,
    m_out,
    a_in,
    m_in,
    b_out,
    b_in,
    r_out,
    r_in,
    c_out,
    c_in,
    load_sem,
    halo_sem,
    s_send,
    s_recv,
    a_send,
    a_recv,
    b_send,
    b_recv,
    r_send,
    r_recv,
    c_send,
    c_recv,
):
    sp, tp = lax.axis_index("sp"), lax.axis_index("tp")
    rows, width = mix_v.shape
    mine, model = stream_v.shape
    half = model // 2
    cols = model // NB
    slots = a_out.shape[1] // NB
    block_sp = EPG // tp_size
    depth = block_sp // 2
    blocks = sp_size // block_sp

    chip, core = sp // 2, lax.rem(sp, 2)
    block, place = chip // depth, lax.rem(chip, depth)
    local = lax.rem(sp, block_sp) * tp_size + tp

    def at(chip_at):
        return {"sp": chip_at * 2 + core, "tp": tp}

    def peer(k):
        other = lax.rem(local + k, EPG)
        return other, {"sp": block * block_sp + other // tp_size, "tp": lax.rem(other, tp_size)}

    low = place < 2
    mod = lax.rem(place, 2)

    def of_block(step, place_at):
        return lax.rem(block + step, blocks) * depth + place_at

    relays = {
        1: (of_block(1, jnp.where(low, 1, 0)), mod),
        2: (of_block(2, jnp.where(low, place + 2, place - 2)), jnp.int32(2)),
        3: (of_block(3, jnp.where(low, 3, 2)), mod),
    }
    side = jnp.where(low, blocks - 1, 1)
    first = jnp.where(mod == 0, 2, 0)
    sources = [
        (of_block(side, first), jnp.where(low, 1, 3)),
        (of_block(side, first + 1), jnp.where(low, 1, 3)),
        (of_block(2, jnp.where(low, place + 2, place - 2)), jnp.int32(2)),
    ]
    after, before = lax.rem(sp + 1, sp_size), lax.rem(sp + sp_size - 1, sp_size)
    right, left = lax.rem(tp + 1, tp_size), lax.rem(tp + tp_size - 1, tp_size)

    def remote(src, dst, send, recv, where):
        return pltpu.make_async_remote_copy(
            src_ref=src, dst_ref=dst, send_sem=send, recv_sem=recv, device_id=where, device_id_type=MESH
        )

    barrier = pltpu.get_barrier_semaphore()

    def greet(where):
        pl.semaphore_signal(barrier, inc=1, device_id=where, device_id_type=MESH)

    for step in (1, 2, 3):
        greet(at(relays[step][0]))
    for source, _ in sources:
        greet(at(source))
    greet({"sp": before, "tp": tp})

    def greet_peer(k, carry):
        greet(peer(k)[1])
        return carry

    lax.fori_loop(1, EPG, greet_peer, 0)

    loads = [
        pltpu.make_async_copy(src, dst, load_sem.at[i])
        for i, (src, dst) in enumerate(
            (
                (mix_hbm, mix_v),
                (gw_hbm.at[0], gw_v),
                (ow_hbm, ow_v),
                (resid_hbm, resid_v),
                (wg_hbm.at[0], wg_v),
                (wu_hbm.at[0], wu_v),
                (wd_hbm.at[0], wd_v),
            )
        )
    ]
    for load in loads:
        load.start()

    first_id, second_id = ids_ref[:, 0:1], ids_ref[:, 1:2]
    lane = iota((mine, 128), 1)
    named_first, named_second = first_id == lane, second_id == lane
    earlier = (iota((mine, mine), 0) > iota((mine, mine), 1)).astype(BF)
    ahead = dot(earlier, (named_first | named_second).astype(BF))
    group = lax.shift_right_logical(first_id, EPG.bit_length() - 1)
    in_group = group == lane
    ahead_group = dot(earlier, in_group.astype(BF))
    rank = jnp.sum(jnp.where(in_group, ahead_group, 0.0), axis=1, keepdims=True).astype(jnp.int32)

    def row_of(ids, named):
        order = jnp.sum(jnp.where(named, ahead, 0.0), axis=1, keepdims=True)
        return (ids - group * EPG).astype(F32) * CAP + order + 1.0

    def thirds(value):
        top = value.astype(BF).astype(F32)
        middle = (value - top).astype(BF).astype(F32)
        return [top, middle, value - top - middle]

    entries = [row_of(first_id, named_first), row_of(second_id, named_second)]
    entries += thirds(rw_ref[:, 0:1]) + thirds(rw_ref[:, 1:2])
    table = jnp.zeros((mine, 128), F32)
    for i, entry in enumerate(entries):
        table = jnp.where(lane == i, entry, table)
    table = table.astype(BF)
    step_of = lax.rem(group - block + blocks, blocks)
    chosen = (step_of * slots + rank == lane).astype(BF)
    for step in range(blocks):
        picked = ((step_of == step) & (rank == lax.rem(lane, slots))).astype(BF)
        m_out[step] = dot_t(table, picked)[0:8]

    loads[0].wait()
    reach = jnp.left_shift(jnp.int32(2), tp)
    doc_row = doc_ref[...]
    sub, lan = iota((rows, rows), 0), iota((rows, rows), 1)
    doc_col = jnp.sum(jnp.where(sub == lan, doc_row, 0).astype(F32), axis=1, keepdims=True)
    doc_row = doc_row.astype(F32)
    member = (doc_col == doc_row) & (sub >= lan) & (sub - lan < reach)
    member = member.astype(F32)
    count = jnp.sum(member, axis=1, keepdims=True)
    total = dot(member.astype(BF), mix_v[...])
    mixed_v[...] = (total / count - mix_v[...].astype(F32)).astype(BF)
    tail = halo_v.shape[0] - HALO
    halo_v[0:tail] = jnp.zeros((tail, width), BF)

    pl.semaphore_wait(barrier, EPG - 1 + 3 + 3 + 1)
    next_dev = {"sp": after, "tp": tp}
    halo = [
        remote(mix_v.at[pl.ds(rows - HALO, HALO)], halo_v.at[pl.ds(tail, HALO)], halo_sem.at[0], halo_sem.at[1], next_dev),
        remote(doc_ref, hdoc_v, halo_sem.at[2], halo_sem.at[3], next_dev),
    ]
    for copy in halo:
        copy.start()
    for copy in halo:
        copy.wait_recv()
    hdoc = hdoc_v[:, rows - 128 :].astype(F32)
    hsub, hlan = iota((HALO, 128), 0), iota((HALO, 128), 1)
    hmember = (doc_col[0:HALO] == hdoc) & (hsub + 128 - hlan < reach) & (sp > 0)
    hmember = hmember.astype(F32)
    hcount = count[0:HALO] + jnp.sum(hmember, axis=1, keepdims=True)
    htotal = total[0:HALO] + dot(hmember.astype(BF), halo_v[...])
    mixed_v[0:HALO] = (htotal / hcount - mix_v[0:HALO].astype(F32)).astype(BF)

    loads[1].wait()
    grouped_v[...] = (dot(mixed_v[...], gw_v[...]) * scale_ref[...]).astype(BF)
    loads[2].wait()

    def part(owner, lo, n):
        piece = grouped_v[pl.ds(pl.multiple_of(owner * mine, mine), mine)]
        return dot(piece, ow_v[:, lo : lo + n])

    opposite = lax.rem(tp + 2, tp_size)
    to_right, to_left = {"sp": sp, "tp": right}, {"sp": sp, "tp": left}
    hops = []
    for i, where in enumerate((to_right, to_left)):
        s1_out[i] = part(opposite, i * half, half).astype(BF)
        copy = remote(s1_out.at[i], s1_in.at[i], s_send.at[i], s_recv.at[i], where)
        copy.start()
        hops.append(copy)
    for i, (owner, where) in enumerate(((right, to_right), (left, to_left))):
        j = 1 - i
        s2_out[i, j] = part(owner, j * half, half).astype(BF)
        copy = remote(s2_out.at[i, j], s2_in.at[i, j], s_send.at[2 + 2 * i + j], s_recv.at[2 + 2 * i + j], where)
        copy.start()
        hops.append(copy)
    sums = [part(right, 0, half), part(left, half, half)]
    for i, where in enumerate((to_right, to_left)):
        hops[i].wait_recv()
        s2_out[i, i] = (sums[i] + s1_in[i].astype(F32)).astype(BF)
        copy = remote(s2_out.at[i, i], s2_in.at[i, i], s_send.at[2 + 3 * i], s_recv.at[2 + 3 * i], where)
        copy.start()
        hops.append(copy)
    own = [part(tp, 0, half), part(tp, half, half)]
    loads[3].wait()
    for copy in hops[2:]:
        copy.wait_recv()
    level = jnp.zeros((mine, 1), F32)
    streams = []
    for j in range(2):
        projected = own[j] + s2_in[0, j].astype(F32) + s2_in[1, j].astype(F32)
        stream = (resid_v[:, j * half : (j + 1) * half].astype(F32) + projected).astype(BF)
        stream_v[:, j * half : (j + 1) * half] = stream
        stream = stream.astype(F32)
        level += jnp.sum(stream * stream, axis=1, keepdims=True)
        streams.append(stream)
    factor = lax.rsqrt(level / model + 1e-06)
    for j in range(2):
        normed = (streams[j] * factor * gain_ref[:, j * half : (j + 1) * half]).astype(BF)
        packed = dot_t(chosen, normed).astype(BF)
        for b in range(NB // 2):
            at_row = (j * (NB // 2) + b) * slots
            for step in range(blocks):
                a_out[step, at_row : at_row + slots] = packed[
                    step * slots : (step + 1) * slots, b * cols : (b + 1) * cols
                ]
    forwards = []
    for step in (1, 3, 2):
        chip_at, slot = relays[step]
        for src, dst, n in ((m_out, m_in, 0), (a_out, a_in, 1)):
            copy = remote(src.at[step], dst.at[slot], a_send.at[step - 1, n], a_recv.at[slot, n], at(chip_at))
            copy.start()
            forwards.append(copy)

    line = iota((EPG * CAP * NB, 128), 0).astype(F32)
    block_of = (iota((1, 128), 1) // slots).astype(F32)

    def hits(meta):
        spots = []
        for i in range(2):
            entry = meta[i : i + 1]
            spots.append(line == jnp.where(entry > 0.0, (entry - 1.0) * NB + block_of, -1.0))
        return spots

    def send_rows(out, into, send, recv, q):
        into[q, local] = out[q, local]

        def one(k, carry):
            other, where = peer(k)
            remote(out.at[q, other], into.at[q, local], send.at[q], recv.at[q], where).start()
            return carry

        lax.fori_loop(1, EPG, one, 0)

    def relay(meta, tokens, q):
        one, two = hits(meta)
        sent = dot((one | two).astype(BF), tokens).astype(BF)
        b_out[q] = sent.reshape(EPG, CAP * NB, cols)
        send_rows(b_out, b_in, b_send, b_recv, q)

    def combine(meta, q):
        drain(r_in.at[q, pl.ds(0, EPG - 1)], r_recv.at[q])
        one, two = hits(meta)
        weigh = [meta[2 + 3 * i : 3 + 3 * i] + meta[3 + 3 * i : 4 + 3 * i] + meta[4 + 3 * i : 5 + 3 * i] for i in range(2)]
        weights = jnp.where(one, weigh[0], 0.0) + jnp.where(two, weigh[1], 0.0)
        high = weights.astype(BF)
        rest = (weights - high.astype(F32)).astype(BF)
        answers = r_in[q].reshape(EPG * CAP * NB, cols)
        return (dot_t(high, answers) + dot_t(rest, answers)).astype(BF)

    many = EPG * CAP
    turn_r, turn_c = iota((many * NB, many * NB), 0), iota((many * NB, many * NB), 1)
    to_blocks = (lax.rem(turn_r, many) * NB + turn_r // many == turn_c).astype(BF)
    to_rows = (lax.rem(turn_c, many) * NB + turn_c // many == turn_r).astype(BF)

    def serve(q):
        drain(b_in.at[q, pl.ds(0, EPG - 1)], b_recv.at[q])
        x = dot(to_blocks, b_in[q].reshape(many * NB, cols)).astype(BF)
        gate = jnp.zeros((many, wg_v.shape[1]), F32)
        up = jnp.zeros((many, wg_v.shape[1]), F32)
        for b in range(NB):
            xb = x[b * many : (b + 1) * many]
            gate += dot(xb, wg_v[b * cols : (b + 1) * cols])
            up += dot(xb, wu_v[b * cols : (b + 1) * cols])
        hidden = (gate * jax.nn.sigmoid(gate) * up).astype(BF)
        answers = [dot(hidden, wd_v[:, b * cols : (b + 1) * cols]).astype(BF) for b in range(NB)]
        served = dot(to_rows, jnp.concatenate(answers, axis=0)).astype(BF)
        r_out[q] = served.reshape(EPG, CAP * NB, cols)
        send_rows(r_out, r_in, r_send, r_recv, q)

    relay(m_out[0], a_out[0], 0)
    for load in loads[4:]:
        load.wait()

    def back(slot):
        source, step = sources[slot]
        return remote(
            c_out.at[slot],
            c_in.at[:, pl.ds(pl.multiple_of(step * slots, slots), slots)],
            c_send.at[slot],
            c_recv.at[step],
            at(source),
        )

    def store_combined(q):
        if q == 0:
            c_in[:, 0:slots] = combine(m_out[0], 0).reshape(NB, slots, cols)
        else:
            c_out[q - 1] = combine(m_in[q - 1], q).reshape(NB, slots, cols)
            back(q - 1).start()

    for q in range(4):
        if q < 3:
            for n, ref in enumerate((m_in, a_in)):
                drain(ref.at[q], a_recv.at[q, n])
            relay(m_in[q], a_in[q], q + 1)
        serve(q)
        if q > 0:
            store_combined(q - 1)
    store_combined(3)

    for step in (1, 2, 3):
        drain(c_in.at[:, pl.ds(step * slots, slots)], c_recv.at[step])
    for b in range(NB):
        total = dot(chosen, c_in[b])
        span = slice(b * cols, (b + 1) * cols)
        out_ref[:, span] = (stream_v[:, span].astype(F32) + total).astype(BF)

    for copy in halo + hops + forwards:
        copy.wait_send()
    for q in range(4):
        drain(b_out.at[q, pl.ds(0, EPG - 1)], b_send.at[q])
        drain(r_out.at[q, pl.ds(0, EPG - 1)], r_send.at[q])
    for slot in range(3):
        back(slot).wait_send()


def shards(mix_in, resid_in, doc_ids, group_weight, pool_scale, out_weight, norm_gain, expert_ids, route_weights, w_gate, w_up, w_down):
    sp_size, tp_size = lax.axis_size("sp"), lax.axis_size("tp")
    rows, width = mix_in.shape
    mine, model = resid_in.shape
    hidden = w_gate.shape[2]
    cols = model // NB
    slots = mine // 2
    steps = sp_size * tp_size // EPG
    anywhere, vmem = pl.BlockSpec(memory_space=pl.ANY), pl.BlockSpec(memory_space=pltpu.VMEM)
    dma = pltpu.SemaphoreType.DMA
    message = (4, EPG, CAP * NB, cols)

    def body(*refs):
        kernel(sp_size, tp_size, *refs)

    return pl.pallas_call(
        body,
        out_shape=jax.ShapeDtypeStruct((mine, model), BF),
        in_specs=[anywhere, anywhere, vmem, anywhere, vmem, anywhere, vmem, vmem, vmem, anywhere, anywhere, anywhere],
        out_specs=vmem,
        scratch_shapes=[
            pltpu.VMEM((rows, width), BF),
            pltpu.VMEM((128, width), BF),
            pltpu.VMEM((1, rows), jnp.int32),
            pltpu.VMEM((mine, model), BF),
            pltpu.VMEM((width, width), BF),
            pltpu.VMEM((width, model), BF),
            pltpu.VMEM((model, hidden), BF),
            pltpu.VMEM((model, hidden), BF),
            pltpu.VMEM((hidden, model), BF),
            pltpu.VMEM((rows, width), BF),
            pltpu.VMEM((rows, width), BF),
            pltpu.VMEM((2, mine, model // 2), BF),
            pltpu.VMEM((2, mine, model // 2), BF),
            pltpu.VMEM((2, 2, mine, model // 2), BF),
            pltpu.VMEM((2, 2, mine, model // 2), BF),
            pltpu.VMEM((mine, model), BF),
            pltpu.VMEM((steps, NB * slots, cols), BF),
            pltpu.VMEM((steps, 8, 128), F32),
            pltpu.VMEM((steps - 1, NB * slots, cols), BF),
            pltpu.VMEM((steps - 1, 8, 128), F32),
            pltpu.VMEM(message, BF),
            pltpu.VMEM(message, BF),
            pltpu.VMEM(message, BF),
            pltpu.VMEM(message, BF),
            pltpu.VMEM((steps - 1, NB, slots, cols), BF),
            pltpu.VMEM((NB, steps * slots, cols), BF),
            dma((7,)),
            dma((4,)),
            dma((6,)),
            dma((6,)),
            dma((3, 2)),
            dma((3, 2)),
            dma((4,)),
            dma((4,)),
            dma((4,)),
            dma((4,)),
            dma((3,)),
            dma((4,)),
        ],
        compiler_params=pltpu.CompilerParams(collective_id=0, has_side_effects=True, vmem_limit_bytes=60 * 1024 * 1024),
    )(
        mix_in,
        resid_in,
        doc_ids.reshape(1, rows),
        group_weight,
        pool_scale.reshape(1, width),
        out_weight,
        norm_gain.reshape(1, model),
        expert_ids,
        route_weights,
        w_gate,
        w_up,
        w_down,
    )


def solution(mesh):
    return jax.shard_map(
        shards,
        mesh=mesh,
        in_specs=(
            P(("grp", "sp"), "tp"),
            P(("grp", "sp", "tp"), None),
            P(("grp", "sp")),
            P("tp", None, None),
            P("tp"),
            P("tp", None),
            P(),
            P(("grp", "sp", "tp"), None),
            P(("grp", "sp", "tp"), None),
            P(("sp", "tp"), None, None),
            P(("sp", "tp"), None, None),
            P(("sp", "tp"), None, None),
        ),
        out_specs=P(("grp", "sp", "tp"), None),
        check_vma=False,
    )
```

time: 217 us -> 122 us (0.56)
  Pallas kernels: 0 us -> 116 us
  blocking collectives: 80.8 us -> 0 us
  waiting for transfers between devices: 78.1 us -> 0 us
  starting transfers between devices: 22.2 us -> 0 us
  matrix products: 12.2 us -> 0 us
  local copies, waits for them, and re-layouts: 14.9 us -> 5.69 us
  other arithmetic: 6.56 us -> 0 us
    pallas_call x0 -> x1, Pallas kernels: none -> 116 us  [shards(): pl.pallas_call(body, out_shape=jax.ShapeDtypeStruct((mine, model), BF), i...]
    all_to_all x1 -> x0, blocking collectives: 80.8 us -> none  [shards(): lax.all_to_all(outbox.reshape(expert_count, capacity, width), ('sp', 'tp'...]
    all_to_all x2 -> x0, waiting for transfers between devices: 78.1 us -> none  [the longest x1 52 us: shards(): lax.all_to_all(served, ('sp', 'tp'), split_axis=0, concat_axis=0, tiled=T...]
    all_to_all x2 -> x0, starting transfers between devices: 15.5 us -> none  [the longest x1 10.8 us: shards(): lax.all_to_all(served, ('sp', 'tp'), split_axis=0, concat_axis=0, tiled=T...]
    dot_general x3 -> x0, matrix products: 12.2 us -> none  [the longest x1 4.71 us: shards(): jnp.dot(grouped, out_weight, preferred_element_type=jnp.float32)]
    ppermute x2 -> x0, starting transfers between devices: 6.74 us -> none  [from_behind(): lax.ppermute(value, axis, [(source, source + steps) for source in range(l...]
    reshape x5 -> x1, local copies, waits for them, and re-layouts: 7.72 us -> 1.28 us  [shards(): pool_scale.reshape(1, width)]
    unnamed x13 -> x3, local copies, waits for them, and re-layouts: 0.12 us -> 4.42 us
  transfers between devices with their start and end apart: 4 -> 0, of which waited for: 2 -> 0; matrix products, arithmetic and copies ran while one was open for 1% -> 0% of each run, Pallas kernels for 0% -> 0%
where the time goes in v1:
time: 122 us
  Pallas kernels  116 us (95%)
  local copies, waits for them, and re-layouts  5.69 us (5%)
    pallas_call x1, Pallas kernels, shards(): pl.pallas_call(body, out_shape=jax.ShapeDtypeStruct((mine, model), BF), i...  116 us
    unnamed x3, local copies, waits for them, and re-layouts  4.42 us

profile of v1, /device:TPU:40, one launch (start us, length us, event | category | flops | bytes accessed | tf_op | source)
XLA Modules:
  0.0 121.9 jit_solution(234216257729905447)
XLA Ops:
  0.0 1.3 %reshape.10.refs_4_ = f32[1,384]{1,0:T(1,128)} reshape(f32[384]{0:T(512)} %param.16) | data formatting | bytes 3072 | tf_op jit(solution)/shard_map/reshape | solution.py:461
  1.3 1.4 %copy.13.refs_7_ = s32[64,2]{1,0:T(8,128)} copy(s32[64,2]{0,1:T(2,128)} %param.19) | data formatting | bytes 1024 | tf_op args[7]
  2.7 1.4 %copy.14.refs_8_ = f32[64,2]{1,0:T(8,128)} copy(f32[64,2]{0,1:T(2,128)} %param.20) | data formatting | bytes 1024 | tf_op args[8]
  4.0 116.2 %shard_map.118 = bf16[64,2048]{1,0:T(8,128)(2,1)} custom-call(bf16[256,384]{1,0:T(8,128)(2,1)} %refs_0_.1, bf16[64,2048]{1,0:T(8,128)(2,1)} %refs_1_.1, s32[1,256]{1,0:T(1,128)} %bitcast.3, bf16[1,384,384]{2,1,0:T(8,128)(2,1)} %refs_3_.1, f32[1,384]{1,0:T(1,128)} %reshape.10.refs_4_, bf16[384,2048]{1,0:T(8,128)(2,1)} %refs_5_.1, f32[1,2048]{1,0:T(1,128)} %bitcast.2, ...), custom_call_target="tpu_custom_call" | custom-call | tf_op jit(solution)/shard_map/pallas_call | solution.py:410
  120.2 1.7 %copy.16 = bf16[64,2048]{1,0:T(8,128)(2,1)} copy(bf16[64,2048]{1,0:T(8,128)(2,1)} %shard_map.118) | data formatting | bytes 524288

commit v2 on v1

--- a/solution.py
+++ b/solution.py
@@ -8,9 +8,13 @@
 MESH = pl.DeviceIdType.MESH
 BF = jnp.bfloat16
 F32 = jnp.float32
+scope = jax.named_scope
 HALO = 16
 EPG = 32
 CAP = 2
+TOP_K = 2
+SENDS = (1, 3, 2)
+ORDER = "L0 L1 F0 X0 L2 F1 X1 C0 L3 F2 X2 C1 F3 X3 C2 C3".split()
 NB = 4
 
 
@@ -166,7 +170,12 @@
     for load in loads:
         load.start()
 
-    first_id, second_id = ids_ref[:, 0:1], ids_ref[:, 1:2]
+    same = iota((mine, mine), 0) == iota((mine, mine), 1)
+
+    def column(row):
+        return jnp.sum(jnp.where(same, row.astype(F32), 0.0), axis=1, keepdims=True)
+
+    first_id, second_id = (column(ids_ref[i : i + 1]).astype(jnp.int32) for i in range(TOP_K))
     lane = iota((mine, 128), 1)
     named_first, named_second = first_id == lane, second_id == lane
     earlier = (iota((mine, mine), 0) > iota((mine, mine), 1)).astype(BF)
@@ -186,7 +195,7 @@
         return [top, middle, value - top - middle]
 
     entries = [row_of(first_id, named_first), row_of(second_id, named_second)]
-    entries += thirds(rw_ref[:, 0:1]) + thirds(rw_ref[:, 1:2])
+    entries += thirds(column(rw_ref[0:1])) + thirds(column(rw_ref[1:2]))
     table = jnp.zeros((mine, 128), F32)
     for i, entry in enumerate(entries):
         table = jnp.where(lane == i, entry, table)
@@ -197,7 +206,8 @@
         picked = ((step_of == step) & (rank == lax.rem(lane, slots))).astype(BF)
         m_out[step] = dot_t(table, picked)[0:8]
 
-    loads[0].wait()
+    with scope("w_mix"):
+        loads[0].wait()
     reach = jnp.left_shift(jnp.int32(2), tp)
     doc_row = doc_ref[...]
     sub, lan = iota((rows, rows), 0), iota((rows, rows), 1)
@@ -211,7 +221,8 @@
     tail = halo_v.shape[0] - HALO
     halo_v[0:tail] = jnp.zeros((tail, width), BF)
 
-    pl.semaphore_wait(barrier, EPG - 1 + 3 + 3 + 1)
+    with scope("w_bar"):
+        pl.semaphore_wait(barrier, EPG - 1 + 3 + 3 + 1)
     next_dev = {"sp": after, "tp": tp}
     halo = [
         remote(mix_v.at[pl.ds(rows - HALO, HALO)], halo_v.at[pl.ds(tail, HALO)], halo_sem.at[0], halo_sem.at[1], next_dev),
@@ -219,8 +230,9 @@
     ]
     for copy in halo:
         copy.start()
-    for copy in halo:
-        copy.wait_recv()
+    with scope("w_halo"):
+        for copy in halo:
+            copy.wait_recv()
     hdoc = hdoc_v[:, rows - 128 :].astype(F32)
     hsub, hlan = iota((HALO, 128), 0), iota((HALO, 128), 1)
     hmember = (doc_col[0:HALO] == hdoc) & (hsub + 128 - hlan < reach) & (sp > 0)
@@ -229,9 +241,11 @@
     htotal = total[0:HALO] + dot(hmember.astype(BF), halo_v[...])
     mixed_v[0:HALO] = (htotal / hcount - mix_v[0:HALO].astype(F32)).astype(BF)
 
-    loads[1].wait()
-    grouped_v[...] = (dot(mixed_v[...], gw_v[...]) * scale_ref[...]).astype(BF)
-    loads[2].wait()
+    with scope("w_gw"):
+        loads[1].wait()
+    grouped_v[...] = (dot(mixed_v[...], gw_v[...]) * scale_ref[...].reshape(1, width)).astype(BF)
+    with scope("w_ow"):
+        loads[2].wait()
 
     def part(owner, lo, n):
         piece = grouped_v[pl.ds(pl.multiple_of(owner * mine, mine), mine)]
@@ -253,15 +267,17 @@
         hops.append(copy)
     sums = [part(right, 0, half), part(left, half, half)]
     for i, where in enumerate((to_right, to_left)):
-        hops[i].wait_recv()
+        with scope(f"w_s1_{i}"):
+            hops[i].wait_recv()
         s2_out[i, i] = (sums[i] + s1_in[i].astype(F32)).astype(BF)
         copy = remote(s2_out.at[i, i], s2_in.at[i, i], s_send.at[2 + 3 * i], s_recv.at[2 + 3 * i], where)
         copy.start()
         hops.append(copy)
     own = [part(tp, 0, half), part(tp, half, half)]
-    loads[3].wait()
-    for copy in hops[2:]:
-        copy.wait_recv()
+    with scope("w_s2"):
+        loads[3].wait()
+        for copy in hops[2:]:
+            copy.wait_recv()
     level = jnp.zeros((mine, 1), F32)
     streams = []
     for j in range(2):
@@ -282,7 +298,7 @@
                     step * slots : (step + 1) * slots, b * cols : (b + 1) * cols
                 ]
     forwards = []
-    for step in (1, 3, 2):
+    for step in SENDS:
         chip_at, slot = relays[step]
         for src, dst, n in ((m_out, m_in, 0), (a_out, a_in, 1)):
             copy = remote(src.at[step], dst.at[slot], a_send.at[step - 1, n], a_recv.at[slot, n], at(chip_at))
@@ -316,7 +332,8 @@
         send_rows(b_out, b_in, b_send, b_recv, q)
 
     def combine(meta, q):
-        drain(r_in.at[q, pl.ds(0, EPG - 1)], r_recv.at[q])
+        with scope(f"w_r{q}"):
+            drain(r_in.at[q, pl.ds(0, EPG - 1)], r_recv.at[q])
         one, two = hits(meta)
         weigh = [meta[2 + 3 * i : 3 + 3 * i] + meta[3 + 3 * i : 4 + 3 * i] + meta[4 + 3 * i : 5 + 3 * i] for i in range(2)]
         weights = jnp.where(one, weigh[0], 0.0) + jnp.where(two, weigh[1], 0.0)
@@ -331,7 +348,8 @@
     to_rows = (lax.rem(turn_c, many) * NB + turn_c // many == turn_r).astype(BF)
 
     def serve(q):
-        drain(b_in.at[q, pl.ds(0, EPG - 1)], b_recv.at[q])
+        with scope(f"w_b{q}"):
+            drain(b_in.at[q, pl.ds(0, EPG - 1)], b_recv.at[q])
         x = dot(to_blocks, b_in[q].reshape(many * NB, cols)).astype(BF)
         gate = jnp.zeros((many, wg_v.shape[1]), F32)
         up = jnp.zeros((many, wg_v.shape[1]), F32)
@@ -343,11 +361,9 @@
         answers = [dot(hidden, wd_v[:, b * cols : (b + 1) * cols]).astype(BF) for b in range(NB)]
         served = dot(to_rows, jnp.concatenate(answers, axis=0)).astype(BF)
         r_out[q] = served.reshape(EPG, CAP * NB, cols)
+
+    def answer(q):
         send_rows(r_out, r_in, r_send, r_recv, q)
-
-    relay(m_out[0], a_out[0], 0)
-    for load in loads[4:]:
-        load.wait()
 
     def back(slot):
         source, step = sources[slot]
@@ -366,30 +382,39 @@
             c_out[q - 1] = combine(m_in[q - 1], q).reshape(NB, slots, cols)
             back(q - 1).start()
 
-    for q in range(4):
-        if q < 3:
-            for n, ref in enumerate((m_in, a_in)):
-                drain(ref.at[q], a_recv.at[q, n])
-            relay(m_in[q], a_in[q], q + 1)
-        serve(q)
-        if q > 0:
-            store_combined(q - 1)
-    store_combined(3)
+    def pass_on(q):
+        if q == 0:
+            relay(m_out[0], a_out[0], 0)
+        else:
+            with scope(f"w_a{q}"):
+                for n, ref in enumerate((m_in, a_in)):
+                    drain(ref.at[q - 1], a_recv.at[q - 1, n])
+            relay(m_in[q - 1], a_in[q - 1], q)
+
+    acts = {"L": pass_on, "F": serve, "X": answer, "C": store_combined}
+    for i, name in enumerate(ORDER):
+        if i == 1:
+            with scope("w_weights"):
+                for load in loads[4:]:
+                    load.wait()
+        acts[name[0]](int(name[1]))
 
     for step in (1, 2, 3):
-        drain(c_in.at[:, pl.ds(step * slots, slots)], c_recv.at[step])
+        with scope(f"w_c{step}"):
+            drain(c_in.at[:, pl.ds(step * slots, slots)], c_recv.at[step])
     for b in range(NB):
         total = dot(chosen, c_in[b])
         span = slice(b * cols, (b + 1) * cols)
         out_ref[:, span] = (stream_v[:, span].astype(F32) + total).astype(BF)
 
-    for copy in halo + hops + forwards:
-        copy.wait_send()
-    for q in range(4):
-        drain(b_out.at[q, pl.ds(0, EPG - 1)], b_send.at[q])
-        drain(r_out.at[q, pl.ds(0, EPG - 1)], r_send.at[q])
-    for slot in range(3):
-        back(slot).wait_send()
+    with scope("w_sends"):
+        for copy in halo + hops + forwards:
+            copy.wait_send()
+        for q in range(4):
+            drain(b_out.at[q, pl.ds(0, EPG - 1)], b_send.at[q])
+            drain(r_out.at[q, pl.ds(0, EPG - 1)], r_send.at[q])
+        for slot in range(3):
+            back(slot).wait_send()
 
 
 def shards(mix_in, resid_in, doc_ids, group_weight, pool_scale, out_weight, norm_gain, expert_ids, route_weights, w_gate, w_up, w_down):
@@ -458,11 +483,11 @@
         resid_in,
         doc_ids.reshape(1, rows),
         group_weight,
-        pool_scale.reshape(1, width),
+        pool_scale,
         out_weight,
         norm_gain.reshape(1, model),
-        expert_ids,
-        route_weights,
+        expert_ids.T,
+        route_weights.T,
         w_gate,
         w_up,
         w_down,

time: 122 us -> 116 us (0.951); the launches traced: 122 us -> 115 us
  local copies, waits for them, and re-layouts: 5.69 us -> 1.67 us
  Pallas kernels: 116 us -> 113 us
    pallas_call x1, Pallas kernels: 116 us -> 113 us  [shards(): pl.pallas_call(body, out_shape=jax.ShapeDtypeStruct((mine, model), BF), i...]
    unnamed x3 -> x1, local copies, waits for them, and re-layouts: 4.42 us -> 1.67 us
    reshape x1 -> x0, local copies, waits for them, and re-layouts: 1.28 us -> none  [shards(): pool_scale.reshape(1, width)]
where the time goes in v2:
time: 116 us; the launch traced here: 115 us
  Pallas kernels  113 us (97%)
  local copies, waits for them, and re-layouts  1.67 us (1%)
    pallas_call x1, Pallas kernels, shards(): pl.pallas_call(body, out_shape=jax.ShapeDtypeStruct((mine, model), BF), i...  113 us

profile of v2, /device:TPU:40, one launch (start us, length us, event | category | flops | bytes accessed | tf_op | source)
XLA Modules:
  0.0 114.5 jit_solution(6919081412982421522)
XLA Ops:
  0.0 112.9 %shard_map.118 = bf16[64,2048]{1,0:T(8,128)(2,1)} custom-call(bf16[256,384]{1,0:T(8,128)(2,1)} %refs_0_.1, bf16[64,2048]{1,0:T(8,128)(2,1)} %refs_1_.1, s32[1,256]{1,0:T(1,128)} %bitcast.5, bf16[1,384,384]{2,1,0:T(8,128)(2,1)} %refs_3_.1, f32[384]{0:T(512)} %refs_4_.1, bf16[384,2048]{1,0:T(8,128)(2,1)} %refs_5_.1, f32[1,2048]{1,0:T(1,128)} %bitcast.4, ...), custom_call_target="tpu_custom_call" | custom-call | tf_op jit(solution)/shard_map/pallas_call | solution.py:435
  112.9 1.7 %copy.14 = bf16[64,2048]{1,0:T(8,128)(2,1)} copy(bf16[64,2048]{1,0:T(8,128)(2,1)} %shard_map.118) | data formatting | bytes 524288

commit v3 on v2

--- a/solution.py
+++ b/solution.py
@@ -315,11 +315,11 @@
             spots.append(line == jnp.where(entry > 0.0, (entry - 1.0) * NB + block_of, -1.0))
         return spots
 
-    def send_rows(out, into, send, recv, q):
+    def send_rows(out, into, send, recv, q, turned=False):
         into[q, local] = out[q, local]
 
         def one(k, carry):
-            other, where = peer(k)
+            other, where = peer(EPG - k if turned else k)
             remote(out.at[q, other], into.at[q, local], send.at[q], recv.at[q], where).start()
             return carry
 
@@ -363,7 +363,7 @@
         r_out[q] = served.reshape(EPG, CAP * NB, cols)
 
     def answer(q):
-        send_rows(r_out, r_in, r_send, r_recv, q)
+        send_rows(r_out, r_in, r_send, r_recv, q, turned=True)
 
     def back(slot):
         source, step = sources[slot]

time: 116 us -> 116 us (level)
  no operation moved by 1% of the time
where the time goes in v3:
time: 116 us
  Pallas kernels  114 us (98%)
  local copies, waits for them, and re-layouts  1.67 us (1%)
    pallas_call x1, Pallas kernels, shards(): pl.pallas_call(body, out_shape=jax.ShapeDtypeStruct((mine, model), BF), i...  114 us

profile of v3, /device:TPU:40, one launch (start us, length us, event | category | flops | bytes accessed | tf_op | source)
XLA Modules:
  0.0 115.5 jit_solution(12864949648602681945)
XLA Ops:
  0.0 113.8 %shard_map.118 = bf16[64,2048]{1,0:T(8,128)(2,1)} custom-call(bf16[256,384]{1,0:T(8,128)(2,1)} %refs_0_.1, bf16[64,2048]{1,0:T(8,128)(2,1)} %refs_1_.1, s32[1,256]{1,0:T(1,128)} %bitcast.5, bf16[1,384,384]{2,1,0:T(8,128)(2,1)} %refs_3_.1, f32[384]{0:T(512)} %refs_4_.1, bf16[384,2048]{1,0:T(8,128)(2,1)} %refs_5_.1, f32[1,2048]{1,0:T(1,128)} %bitcast.4, ...), custom_call_target="tpu_custom_call" | custom-call | tf_op jit(solution)/shard_map/pallas_call | solution.py:435
  113.8 1.7 %copy.14 = bf16[64,2048]{1,0:T(8,128)(2,1)} copy(bf16[64,2048]{1,0:T(8,128)(2,1)} %shard_map.118) | data formatting | bytes 524288
